TPU v7x, 32 devices: a whole 2x2x4 slice. The times are simulated.
32 devices in a mesh: ep: 32 (over z, y, x, core).
Axes of the slice: x: 2, y: 2, z: 4, core: 2. Of those that a mesh axis runs over, the one named last changes fastest.
Arguments:
- tokens: bfloat16 [256, 2048], P('ep'), may hold values from -6 to 6
- cache_keys: bfloat16 [256, 1024, 128], P('ep'), may hold values from -80 to 80
- cache_values: bfloat16 [256, 1024, 128], P('ep'), may hold values from -6 to 6
- cum_gates: float32 [256, 1024, 2], P('ep'), may hold values from -1024 to 0, as said below
- lengths: int32 [256], P('ep'), may hold values from 128 to 1024
- query_weight: bfloat16 [2048, 2048], replicated, may hold values from -0.125 to 0.125
- key_weight: bfloat16 [2048, 128], replicated, may hold values from -0.125 to 0.125
- value_weight: bfloat16 [2048, 128], replicated, may hold values from -0.125 to 0.125
- forget_weight: bfloat16 [2048, 2], replicated, may hold values from -0.125 to 0.125
- out_weight: bfloat16 [2048, 2048], P('ep'), may hold values from -1 to 1
- norm_gain: float32 [2, 2048], replicated, may hold values from 0.1 to 1.9
- norm_bias: float32 [2, 2048], replicated, may hold values from -1 to 1
- dense_gate_weight: bfloat16 [2048, 5632], P(None, 'ep'), may hold values from -0.125 to 0.125
- dense_up_weight: bfloat16 [2048, 5632], P(None, 'ep'), may hold values from -0.125 to 0.125
- dense_down_weight: bfloat16 [5632, 2048], P('ep'), may hold values from -0.078125 to 0.078125
- dense_scale: float32 [2048], replicated, may hold values from 0.2 to 1.5
- expert_gate_weight: bfloat16 [2048, 57344], P(None, 'ep'), may hold values from -0.125 to 0.125
- expert_up_weight: bfloat16 [2048, 57344], P(None, 'ep'), may hold values from -0.125 to 0.125
- expert_down_weight: bfloat16 [57344, 2048], P('ep'), may hold values from -0.0625 to 0.0625
- routes: int32 [256, 2], replicated, may hold values from 0 to 7, all different within a row; in each aligned block of 8 rows (0 to 7, 8 to 15, ...) at most 3 rows name the same one
- route_weights: float32 [256, 2], replicated, may hold values from 0.2 to 1
Outputs:
- output: bfloat16 [256, 2048], P('ep')
Inputs may be any that keep to these rules, and one draw needn't show every extreme that they name: `routes`: each row names 2 different experts; the rows of one device (8 aligned rows) name one expert at most 3 times. `cum_gates`: non-increasing along positions.
All inputs are finite; a program needn't handle non-finite values.
Results may differ from a plain program's by a relative error of at most 0.012.
Values may be sent and summed in bfloat16 or wider, within the bound.
A program may use at most 128 MiB of HBM per device.

v0:
```python
import functools
import jax
import jax.numpy as jnp
from jax import lax
from jax.experimental import pallas as pl
from jax.experimental.pallas import tpu as pltpu
from jax.sharding import PartitionSpec as P

EXPERTS = 8
MESH = pl.DeviceIdType.MESH

residual_scale = 1.4142135
norm_eps = 1e-05


def layer_norm(values, gain_row, shift_row):
    centre = jnp.mean(values, axis=-1, keepdims=True)
    centred = values - centre
    spread = jnp.mean(centred * centred, axis=-1, keepdims=True)
    return (centred * lax.rsqrt(spread + norm_eps) * gain_row + shift_row).astype(jnp.bfloat16)


def attend(
    heads, kv_count, tokens_ref, query_weight_ref, key_weight_ref, value_weight_ref,
    forget_ref, keys_ref, values_ref, gates_ref, lengths_ref, query_ref, rows_ref, waits, parts,
):
    seqs, model = tokens_ref.shape
    width = key_weight_ref.shape[1]
    head_dim = width // kv_count
    grouped = heads // kv_count
    cache_len = keys_ref.shape[1]
    ratio_value = head_dim ** (-0.5)
    tokens = tokens_ref[...]
    wide = tokens.astype(jnp.float32)
    fresh_gate = jax.nn.log_sigmoid(
        jnp.concatenate(
            [
                jnp.sum(wide * forget_ref[j:j + 1, :].astype(jnp.float32), axis=1, keepdims=True)
                for j in range(kv_count)
            ],
            axis=1,
        )
    )
    waits["keys"]()
    fresh_key = jnp.dot(tokens, key_weight_ref[...], preferred_element_type=jnp.float32)
    fresh_key = fresh_key.astype(jnp.bfloat16).astype(jnp.float32)
    fresh_value = jnp.dot(tokens, value_weight_ref[...], preferred_element_type=jnp.float32)
    fresh_value = fresh_value.astype(jnp.bfloat16).astype(jnp.float32)
    pieces = waits["pieces"]
    piece = model // pieces
    for i in range(pieces):
        waits["query"](i)
        part = jnp.dot(
            tokens, query_weight_ref[:, i * piece:(i + 1) * piece], preferred_element_type=jnp.float32
        ).astype(jnp.bfloat16).astype(jnp.float32)
        for h in range(piece // head_dim):
            head = i * (piece // head_dim) + h
            group = head // grouped
            fields = [jnp.zeros((seqs, head_dim), jnp.float32)] * kv_count
            fields[group] = part[:, h * head_dim:(h + 1) * head_dim]
            query_ref[head * seqs:(head + 1) * seqs, :] = jnp.concatenate(fields, axis=1)
    waits["caches"]()
    positions = lax.broadcasted_iota(jnp.int32, (kv_count, cache_len), 1)
    row_group = lax.broadcasted_iota(jnp.int32, (heads, 1), 0) // grouped
    lanes = rows_ref.shape[1]
    share = head_dim // parts
    for b in range(seqs):
        length = lengths_ref[b]
        gates = gates_ref[b]
        latest = jnp.sum(jnp.where(positions == length - 1, gates, 0.0), axis=1, keepdims=True)
        offsets = jnp.where(positions < length, latest - gates, -jnp.inf)
        spread = offsets[0:1] + fresh_gate[b:b + 1, 0:1]
        spread = jnp.broadcast_to(spread, (heads, cache_len))
        for j in range(1, kv_count):
            spread = jnp.where(row_group == j, offsets[j:j + 1] + fresh_gate[b:b + 1, j:j + 1], spread)
        queries = query_ref[pl.ds(b, heads, stride=seqs), :]
        past = lax.dot_general(
            queries.astype(jnp.bfloat16), keys_ref[b], (((1,), (1,)), ((), ())),
            preferred_element_type=jnp.float32,
        )
        past = past * ratio_value + spread
        self_part = ratio_value * jnp.sum(queries * fresh_key[b:b + 1], axis=1, keepdims=True)
        highest = jnp.maximum(jnp.max(past, axis=1, keepdims=True), self_part)
        past_exp = jnp.exp(past - highest)
        own_exp = jnp.exp(self_part - highest)
        denominator = jnp.sum(past_exp, axis=1, keepdims=True) + own_exp
        past_weight = (past_exp / denominator).astype(jnp.bfloat16)
        own_weight = (own_exp / denominator).astype(jnp.bfloat16).astype(jnp.float32)
        mixed = jnp.dot(past_weight, values_ref[b], preferred_element_type=jnp.float32)
        mixed = mixed + own_weight * fresh_value[b:b + 1]
        mixed = jnp.concatenate(
            [
                mixed[j * grouped:(j + 1) * grouped, j * head_dim:(j + 1) * head_dim]
                for j in range(kv_count)
            ],
            axis=0,
        )
        for p in range(parts):
            block = mixed[:, p * share:(p + 1) * share]
            if share < lanes:
                block = jnp.concatenate([block, jnp.zeros((heads, lanes - share), jnp.float32)], axis=1)
            rows_ref[pl.ds(p * seqs + b, heads, stride=parts * seqs), :] = block


def factors_of(count):
    found = [2]
    rest = count // 2
    while rest > 1:
        step = 4 if rest % 4 == 0 else rest
        found.append(step)
        rest //= step
    return found


def orders_of(stages):
    far = list(range(1, stages))
    return [[0] + far, [0] + far[::-1]]


def step_shapes(factors, order, rows, width):
    left = list(range(len(factors)))[::-1]
    shapes = []
    for axis in order:
        left = [other for other in left if other != axis]
        lead = tuple(factors[other] for other in left)
        shapes.append(((factors[axis] - 1,) + lead + (rows, width), lead + (rows, width)))
    return shapes


def kernel(
    count, factors, orders, widths, heads,
    tokens_ref, gates_ref, lengths_ref, forget_ref, gain_ref, bias_ref, scale_ref,
    routes_ref, shares_ref, query_hbm, key_hbm, value_hbm, keys_hbm, values_hbm, out_hbm,
    gate_hbm, up_hbm, down_hbm, dense_gate_hbm, dense_up_hbm, dense_down_hbm,
    result_ref, *scratch,
):
    pool = list(scratch)
    take = lambda amount: [pool.pop(0) for _ in range(amount)]
    gate_ref, up_ref, down_ref, dense_gate_ref, dense_up_ref, dense_down_ref, load_sem = take(7)
    query_weight_ref, key_weight_ref, value_weight_ref, keys_ref, values_ref, out_weight_ref, early_sem = take(7)
    query_ref, attended_rows_ref, attended_ref, share_ref = take(4)
    mixed_ref, mixed_send, mixed_recv, rows_ref, hidden_ref, dense_ref, settled_ref = take(7)
    stages = len(factors)
    chunks = len(orders)
    exchanges = []
    for _ in range(2):
        per_chunk = []
        for c in range(chunks):
            start = take(1)[0]
            lands = take(stages)
            sums = take(stages - 1)
            per_chunk.append((start, lands, sums))
        exchanges.append((per_chunk, take(2)))
    gathered = take(chunks)
    gather_send, gather_recv = take(2)
    total_rows, model = rows_ref.shape
    seqs = tokens_ref.shape[0]

    me = lax.axis_index("ep")
    coords, strides, rest, stride = [], [], me, 1
    for factor in factors:
        coords.append(lax.rem(rest, factor))
        strides.append(stride)
        rest = rest // factor
        stride *= factor

    def partner(axis, k):
        other = lax.rem(coords[axis] + k, factors[axis])
        return other, me + (other - coords[axis]) * strides[axis]

    sources = (gate_hbm, up_hbm, down_hbm, dense_gate_hbm, dense_up_hbm, dense_down_hbm)
    targets = (gate_ref, up_ref, down_ref, dense_gate_ref, dense_up_ref, dense_down_ref)
    loads = [
        pltpu.make_async_copy(source, target, load_sem.at[i])
        for i, (source, target) in enumerate(zip(sources, targets))
    ]
    barrier = pltpu.get_barrier_semaphore()

    @pl.loop(1, count)
    def _(k):
        pl.semaphore_signal(
            barrier, inc=1, device_id=(lax.rem(me + k, count),), device_id_type=MESH
        )

    model_width = tokens_ref.shape[1]
    pieces = 4
    piece = model_width // pieces
    early = [
        pltpu.make_async_copy(source, target, early_sem.at[i])
        for i, (source, target) in enumerate(
            [(key_hbm, key_weight_ref), (value_hbm, value_weight_ref)]
            + [
                (
                    query_hbm.at[:, pl.ds(i * piece, piece)],
                    query_weight_ref.at[:, pl.ds(i * piece, piece)],
                )
                for i in range(pieces)
            ]
            + [(keys_hbm, keys_ref), (values_hbm, values_ref), (out_hbm, out_weight_ref)]
        )
    ]
    for copy in early:
        copy.start()

    def wait_all(some):
        for copy in some:
            copy.wait()

    def wait_caches():
        for load in loads:
            load.start()
        wait_all(early[2 + pieces:])

    waits = {
        "keys": lambda: wait_all(early[:2]),
        "query": lambda i: early[2 + i].wait(),
        "pieces": pieces,
        "caches": wait_caches,
    }
    kv_count = gates_ref.shape[1]
    attend(
        heads, kv_count, tokens_ref, query_weight_ref, key_weight_ref, value_weight_ref,
        forget_ref, keys_ref, values_ref, gates_ref, lengths_ref, query_ref,
        attended_rows_ref, waits, count // heads,
    )
    attended_ref[...] = attended_rows_ref[...].reshape(attended_ref.shape).astype(jnp.bfloat16)
    pl.semaphore_wait(barrier, count - 1)

    def mixed_copy(k):
        to = lax.rem(me + k, count)
        return pltpu.make_async_remote_copy(
            src_ref=attended_ref.at[to], dst_ref=mixed_ref.at[me],
            send_sem=mixed_send.at[k - 1], recv_sem=mixed_recv.at[k - 1],
            device_id=(to,), device_id_type=MESH,
        )

    @pl.loop(1, count)
    def _(k):
        mixed_copy(k).start()

    mixed_ref[me] = attended_ref[me]
    own_expert = me // (count // EXPERTS)
    row_tile = min(total_rows, 256)
    diagonal = lax.broadcasted_iota(jnp.int32, (row_tile, row_tile), 0) == lax.broadcasted_iota(
        jnp.int32, (row_tile, row_tile), 1
    )
    for i in range(total_rows // row_tile):
        at = slice(i * row_tile, (i + 1) * row_tile)
        chosen = jnp.sum(
            jnp.where(routes_ref[:, at] == own_expert, shares_ref[:, at], 0.0), axis=0, keepdims=True
        )
        share_ref[at, :] = jnp.sum(jnp.where(diagonal, chosen, 0.0), axis=1, keepdims=True)

    @pl.loop(1, count)
    def _(k):
        mixed_copy(k).wait()

    def at_axis(left, axis, index):
        return tuple(index if other == axis else slice(None) for other in left)

    def exchanger(exchange):
        per_chunk, (send_sem, recv_sem) = exchange
        current = [entry[0] for entry in per_chunk]
        left = [list(range(stages))[::-1] for _ in orders]
        flying = [None] * chunks
        finished = [None] * chunks

        def launch(c, stage):
            axis = orders[c][stage]
            copies = []
            for k in range(1, factors[axis]):
                other, device = partner(axis, k)
                copy = pltpu.make_async_remote_copy(
                    src_ref=current[c].at[at_axis(left[c], axis, other)],
                    dst_ref=per_chunk[c][1][stage].at[k - 1],
                    send_sem=send_sem.at[c, stage, k - 1],
                    recv_sem=recv_sem.at[c, stage, k - 1],
                    device_id=(device,), device_id_type=MESH,
                )
                copy.start()
                copies.append(copy)
            flying[c] = copies

        def advance(c, stage):
            axis = orders[c][stage]
            for copy in flying[c]:
                copy.wait()
            landed = per_chunk[c][1][stage]
            own = current[c][at_axis(left[c], axis, coords[axis])].astype(jnp.float32)
            for k in range(factors[axis] - 1):
                own = own + landed[k].astype(jnp.float32)
            left[c] = [other for other in left[c] if other != axis]
            if stage == stages - 1:
                finished[c] = own
            else:
                current[c] = per_chunk[c][2][stage]
                current[c][...] = own.astype(jnp.bfloat16)
                launch(c, stage + 1)

        def finish():
            for stage in range(stages):
                for c in range(chunks):
                    if stage or c:
                        advance(c, stage)
            return jnp.concatenate(finished, axis=-1)

        def computed(c):
            launch(c, 0)
            if c == 1:
                advance(0, 0)

        return computed, finish

    def place(start_ref, first, value, column, span):
        blocks = value.shape[0] // seqs
        lead = start_ref.shape[:-2]
        flat = value.reshape(blocks, seqs, span).astype(jnp.bfloat16)
        inner = lead[1:]
        size = 1
        for factor in inner:
            size *= factor
        whole = blocks // size
        start_ref[pl.ds(first * whole, whole), ..., column] = flat.reshape((whole,) + inner + (seqs, span))

    tile = min(total_rows, 256)
    tiles = total_rows // tile
    span = 256
    mixed_per_tile = tile // seqs
    out_rows = out_weight_ref.shape[0]
    computed, finish = exchanger(exchanges[0])

    per_chunk = exchanges[0][0]
    begin = 0
    for c in range(chunks):
        @pl.loop(0, tiles * (widths[c] // span))
        def _(step):
            row = step // (widths[c] // span)
            column = pl.multiple_of(lax.rem(step, widths[c] // span) * span, span)
            left_side = mixed_ref[pl.ds(row * mixed_per_tile, mixed_per_tile)].astype(jnp.float32)
            left_side = left_side.reshape(tile, mixed_ref.shape[2])[:, :out_rows].astype(jnp.bfloat16)
            part = jnp.dot(
                left_side, out_weight_ref[:, pl.ds(pl.multiple_of(begin + column, span), span)],
                preferred_element_type=jnp.float32,
            )
            place(per_chunk[c][0], row, part, pl.ds(column, span), span)
        begin += widths[c]
        computed(c)

    projected = finish()
    settled = layer_norm(
        residual_scale * tokens_ref[...].astype(jnp.float32) + projected, gain_ref[0:1], bias_ref[0:1]
    )
    settled_ref[...] = settled

    mine = tuple(coords[axis] for axis in range(stages)[::-1])
    begin = 0
    for c in range(chunks):
        gathered[c][mine] = settled[:, begin:begin + widths[c]]
        begin += widths[c]
    flying = [None] * chunks
    have = [[] for _ in orders]

    def spread(c, stage):
        axis = orders[c][::-1][stage]
        index = tuple(
            slice(None) if other in have[c] else coords[other] for other in range(stages)[::-1]
        )
        copies = []
        for k in range(1, factors[axis]):
            _, device = partner(axis, k)
            copy = pltpu.make_async_remote_copy(
                src_ref=gathered[c].at[index], dst_ref=gathered[c].at[index],
                send_sem=gather_send.at[c, stage, k - 1], recv_sem=gather_recv.at[c, stage, k - 1],
                device_id=(device,), device_id_type=MESH,
            )
            copy.start()
            copies.append(copy)
        flying[c] = copies
        have[c].append(axis)

    for c in range(chunks):
        spread(c, 0)
    for stage in range(stages):
        for c in range(chunks):
            for copy in flying[c]:
                copy.wait()
            if stage < stages - 1:
                spread(c, stage + 1)
    begin = 0
    for c in range(chunks):
        block = gathered[c][...].astype(jnp.float32).reshape(total_rows, widths[c])
        rows_ref[:, begin:begin + widths[c]] = block.astype(jnp.bfloat16)
        begin += widths[c]

    for i in (0, 1, 3, 4):
        loads[i].wait()
    units = gate_ref.shape[1]
    unit_span = span if units % span == 0 else units

    def hidden_of(inputs, gates, ups, depth=0):
        contract = (((1,), (depth,)), ((), ()))
        gate_val = lax.dot_general(inputs, gates, contract, preferred_element_type=jnp.float32)
        up_val = lax.dot_general(inputs, ups, contract, preferred_element_type=jnp.float32)
        return (jax.nn.silu(gate_val) * up_val).astype(jnp.bfloat16)

    @pl.loop(0, tiles)
    def _(row):
        at_rows = pl.ds(pl.multiple_of(row * tile, tile), tile)
        dense_ref[at_rows, :] = hidden_of(
            rows_ref[at_rows, :], dense_gate_ref[...], dense_up_ref[...], 1
        )
        if unit_span == units:
            hidden_ref[at_rows, :] = hidden_of(rows_ref[at_rows, :], gate_ref[...], up_ref[...])
        else:
            @pl.loop(0, units // unit_span)
            def _(step):
                at_units = pl.ds(pl.multiple_of(step * unit_span, unit_span), unit_span)
                hidden_ref[at_rows, at_units] = hidden_of(
                    rows_ref[at_rows, :], gate_ref[:, at_units], up_ref[:, at_units]
                )

    for i in (2, 5):
        loads[i].wait()
    per_chunk = exchanges[1][0]
    computed, finish = exchanger(exchanges[1])
    begin = 0
    for c in range(chunks):
        @pl.loop(0, tiles * (widths[c] // span))
        def _(step):
            row = step // (widths[c] // span)
            column = pl.multiple_of(lax.rem(step, widths[c] // span) * span, span)
            at_columns = pl.ds(pl.multiple_of(begin + column, span), span)
            at_rows = pl.ds(pl.multiple_of(row * tile, tile), tile)
            expert_out = jnp.dot(
                hidden_ref[at_rows, :], down_ref[:, at_columns], preferred_element_type=jnp.float32
            )
            dense_out = jnp.dot(
                dense_ref[at_rows, :], dense_down_ref[:, at_columns], preferred_element_type=jnp.float32
            )
            part = share_ref[at_rows, :] * expert_out + scale_ref[:, at_columns] * dense_out
            place(per_chunk[c][0], row, part, pl.ds(column, span), span)
        begin += widths[c]
        computed(c)

    ffn = finish()
    result_ref[...] = layer_norm(
        residual_scale * settled_ref[...].astype(jnp.float32) + ffn, gain_ref[1:2], bias_ref[1:2]
    )


def whole_step(
    count, heads, tokens, gates, lengths, forget, norm_gain, norm_bias, dense_scale, routes, shares,
    query_weight, key_weight, value_weight, cache_keys, cache_values, out_weight,
    expert_gate, expert_up, expert_down, dense_gate, dense_up, dense_down,
):
    seqs, model = tokens.shape
    factors = factors_of(count)
    stages = len(factors)
    orders = orders_of(stages)
    narrow = model * 3 // 8
    widths = [model - narrow, narrow]
    total_rows = count * seqs
    lead = tuple(factors[::-1])
    scratch = [
        pltpu.VMEM(array.shape, array.dtype)
        for array in (expert_gate, expert_up, expert_down, dense_gate, dense_up, dense_down)
    ]
    scratch += [
        pltpu.SemaphoreType.DMA((6,)),
        *[
            pltpu.VMEM(array.shape, array.dtype)
            for array in (query_weight, key_weight, value_weight, cache_keys, cache_values, out_weight)
        ],
        pltpu.SemaphoreType.DMA((9,)),
        pltpu.VMEM((heads * seqs, key_weight.shape[1]), jnp.float32),
        pltpu.VMEM((total_rows, 128), jnp.float32),
        pltpu.VMEM((count, seqs, 128), jnp.bfloat16),
        pltpu.VMEM((total_rows, 1), jnp.float32),
        pltpu.VMEM((count, seqs, 128), jnp.bfloat16),
        pltpu.SemaphoreType.DMA((count - 1,)),
        pltpu.SemaphoreType.DMA((count - 1,)),
        pltpu.VMEM((total_rows, model), jnp.bfloat16),
        pltpu.VMEM((total_rows, expert_gate.shape[1]), jnp.bfloat16),
        pltpu.VMEM((total_rows, dense_gate.shape[0]), jnp.bfloat16),
        pltpu.VMEM((seqs, model), jnp.bfloat16),
    ]
    most = max(factors) - 1
    for _ in range(2):
        for order, width in zip(orders, widths):
            shapes = step_shapes(factors, order, seqs, width)
            scratch.append(pltpu.VMEM(lead + (seqs, width), jnp.bfloat16))
            scratch += [pltpu.VMEM(shape[0], jnp.bfloat16) for shape in shapes]
            scratch += [pltpu.VMEM(shape[1], jnp.bfloat16) for shape in shapes[:-1]]
        scratch += [pltpu.SemaphoreType.DMA((len(orders), stages, most))] * 2
    scratch += [pltpu.VMEM(lead + (seqs, width), jnp.bfloat16) for width in widths]
    scratch += [pltpu.SemaphoreType.DMA((len(orders), stages, most))] * 2
    vmem = pl.BlockSpec(memory_space=pltpu.VMEM)
    away = pl.BlockSpec(memory_space=pl.ANY)
    return pl.pallas_call(
        functools.partial(kernel, count, factors, orders, widths, heads),
        out_shape=jax.ShapeDtypeStruct((seqs, model), jnp.bfloat16),
        in_specs=[vmem] * 2
        + [pl.BlockSpec(memory_space=pltpu.SMEM)]
        + [vmem] * 6
        + [away] * 12,
        out_specs=vmem,
        scratch_shapes=scratch,
        compiler_params=pltpu.CompilerParams(
            collective_id=0, has_side_effects=True, vmem_limit_bytes=60 * 1024 * 1024
        ),
        name="whole_step",
    )(
        tokens, gates, lengths, forget, norm_gain, norm_bias, dense_scale, routes, shares,
        query_weight, key_weight, value_weight, cache_keys, cache_values, out_weight,
        expert_gate, expert_up, expert_down, dense_gate, dense_up, dense_down,
    )


def local(
    tokens,
    cache_keys,
    cache_values,
    cum_gates,
    lengths,
    query_weight,
    key_weight,
    value_weight,
    forget_weight,
    out_weight,
    norm_gain,
    norm_bias,
    dense_gate_weight,
    dense_up_weight,
    dense_down_weight,
    dense_scale,
    expert_gate_weight,
    expert_up_weight,
    expert_down_weight,
    routes,
    route_weights,
):
    count = lax.axis_size("ep")
    head_dim = key_weight.shape[1] // cum_gates.shape[2]
    heads = query_weight.shape[1] // head_dim
    return whole_step(
        count, heads, tokens, jnp.transpose(cum_gates, (0, 2, 1)), lengths, forget_weight.T,
        norm_gain, norm_bias, dense_scale[None, :], routes.T, route_weights.T,
        query_weight, key_weight, value_weight, cache_keys, cache_values, out_weight,
        expert_gate_weight, expert_up_weight, expert_down_weight,
        dense_gate_weight.T, dense_up_weight.T, dense_down_weight,
    )


def solution(mesh):
    return jax.shard_map(
        local,
        mesh=mesh,
        in_specs=(
            P("ep", None),
            P("ep", None, None),
            P("ep", None, None),
            P("ep", None, None),
            P("ep"),
            P(),
            P(),
            P(),
            P(),
            P("ep", None),
            P(),
            P(),
            P(None, "ep"),
            P(None, "ep"),
            P("ep", None),
            P(),
            P(None, "ep"),
            P(None, "ep"),
            P("ep", None),
            P(),
            P(),
        ),
        out_specs=P("ep", None),
        check_vma=False,
    )
```

profile of v0, /device:TPU:0, one launch (start us, length us, event | category | flops | bytes accessed | tf_op | source)
XLA Modules:
  0.0 64.2 jit_solution(4643922062803143027)
XLA Ops:
  0.0 62.8 %whole_step.1 = bf16[8,2048]{1,0:T(8,128)(2,1)} custom-call(bf16[8,2048]{1,0:T(8,128)(2,1)} %tokens_ref.1, f32[8,2,1024]{2,1,0:T(2,128)} %bitcast.9, s32[8]{0:T(128)} %lengths_ref.1, bf16[2,2048]{1,0:T(2,128)(2,1)} %bitcast.10, f32[2,2048]{1,0:T(2,128)} %gain_ref.1, f32[2,2048]{1,0:T(2,128)} %bias_ref.1, f32[1,2048]{1,0:T(1,128)} %bitcast.11, ...), custom_call_target="tpu_custom_call" | custom-call | tf_op jit(solution)/shard_map/whole_step/pallas_call | solution.py:499
  62.8 1.4 %copy.23 = bf16[8,2048]{1,0:T(8,128)(2,1)} copy(bf16[8,2048]{1,0:T(8,128)(2,1)} %whole_step.1) | data formatting | bytes 65536
where the time goes:
time: 64.4 us; the launch traced here: 64.2 us
  Pallas kernels  62.8 us (98%)
  local copies, waits for them, and re-layouts  1.38 us (2%)
    pallas_call x1, Pallas kernels, whole_step(): pl.pallas_call(functools.partial(kernel, count, factors, orders, widths,...  62.8 us
    unnamed x1, local copies, waits for them, and re-layouts  1.38 us

commit v1 on v0

v1 whole, which is shorter than its diff:
```python
import functools
import jax
import jax.numpy as jnp
from jax import lax
from jax.experimental import pallas as pl
from jax.experimental.pallas import tpu as pltpu
from jax.sharding import PartitionSpec as P

EXPERTS = 8
CAP = 3
MESH = pl.DeviceIdType.MESH

residual_scale = 1.4142135
norm_eps = 1e-05


def layer_norm(values, gain_row, shift_row):
    centre = jnp.mean(values, axis=-1, keepdims=True)
    centred = values - centre
    spread = jnp.mean(centred * centred, axis=-1, keepdims=True)
    return (centred * lax.rsqrt(spread + norm_eps) * gain_row + shift_row).astype(jnp.bfloat16)


def attend(
    heads, kv_count, tokens_ref, query_weight_ref, key_weight_ref, value_weight_ref,
    forget_ref, keys_ref, values_ref, gates_ref, lengths_ref, query_ref, rows_ref, waits, parts,
):
    seqs, model = tokens_ref.shape
    width = key_weight_ref.shape[1]
    head_dim = width // kv_count
    grouped = heads // kv_count
    cache_len = keys_ref.shape[1]
    ratio_value = head_dim ** (-0.5)
    waits["small"]()
    tokens = tokens_ref[...]
    wide = tokens.astype(jnp.float32)
    fresh_gate = jax.nn.log_sigmoid(
        jnp.concatenate(
            [
                jnp.sum(wide * forget_ref[j:j + 1, :].astype(jnp.float32), axis=1, keepdims=True)
                for j in range(kv_count)
            ],
            axis=1,
        )
    )
    waits["keys"]()
    fresh_key = jnp.dot(tokens, key_weight_ref[...], preferred_element_type=jnp.float32)
    fresh_key = fresh_key.astype(jnp.bfloat16).astype(jnp.float32)
    fresh_value = jnp.dot(tokens, value_weight_ref[...], preferred_element_type=jnp.float32)
    fresh_value = fresh_value.astype(jnp.bfloat16).astype(jnp.float32)
    pieces = waits["pieces"]
    piece = model // pieces
    for i in range(pieces):
        waits["query"](i)
        part = jnp.dot(
            tokens, query_weight_ref[:, i * piece:(i + 1) * piece], preferred_element_type=jnp.float32
        ).astype(jnp.bfloat16).astype(jnp.float32)
        for h in range(piece // head_dim):
            head = i * (piece // head_dim) + h
            group = head // grouped
            fields = [jnp.zeros((seqs, head_dim), jnp.float32)] * kv_count
            fields[group] = part[:, h * head_dim:(h + 1) * head_dim]
            query_ref[head * seqs:(head + 1) * seqs, :] = jnp.concatenate(fields, axis=1)
    positions = lax.broadcasted_iota(jnp.int32, (kv_count, cache_len), 1)
    row_group = lax.broadcasted_iota(jnp.int32, (heads, 1), 0) // grouped
    lanes = rows_ref.shape[1]
    share = head_dim // parts
    batch = seqs // waits["batches"]
    for b in range(seqs):
        if b % batch == 0:
            waits["caches"](b // batch)
        length = lengths_ref[:, b:b + 1]
        gates = gates_ref[b]
        latest = jnp.sum(jnp.where(positions == length - 1, gates, 0.0), axis=1, keepdims=True)
        offsets = jnp.where(positions < length, latest - gates, -jnp.inf)
        spread = offsets[0:1] + fresh_gate[b:b + 1, 0:1]
        spread = jnp.broadcast_to(spread, (heads, cache_len))
        for j in range(1, kv_count):
            spread = jnp.where(row_group == j, offsets[j:j + 1] + fresh_gate[b:b + 1, j:j + 1], spread)
        queries = query_ref[pl.ds(b, heads, stride=seqs), :]
        past = lax.dot_general(
            queries.astype(jnp.bfloat16), keys_ref[b], (((1,), (1,)), ((), ())),
            preferred_element_type=jnp.float32,
        )
        past = past * ratio_value + spread
        self_part = ratio_value * jnp.sum(queries * fresh_key[b:b + 1], axis=1, keepdims=True)
        highest = jnp.maximum(jnp.max(past, axis=1, keepdims=True), self_part)
        past_exp = jnp.exp(past - highest)
        own_exp = jnp.exp(self_part - highest)
        denominator = jnp.sum(past_exp, axis=1, keepdims=True) + own_exp
        mixed = jnp.dot(past_exp.astype(jnp.bfloat16), values_ref[b], preferred_element_type=jnp.float32)
        mixed = (mixed + own_exp * fresh_value[b:b + 1]) / denominator
        mixed = jnp.concatenate(
            [
                mixed[j * grouped:(j + 1) * grouped, j * head_dim:(j + 1) * head_dim]
                for j in range(kv_count)
            ],
            axis=0,
        )
        for p in range(parts):
            block = mixed[:, p * share:(p + 1) * share]
            if share < lanes:
                block = jnp.concatenate([block, jnp.zeros((heads, lanes - share), jnp.float32)], axis=1)
            rows_ref[pl.ds(p * seqs + b, heads, stride=parts * seqs), :] = block


def factors_of(count):
    found = [2]
    rest = count // 2
    while rest > 1:
        step = 4 if rest % 4 == 0 else rest
        found.append(step)
        rest //= step
    return found


def orders_of(stages):
    far = list(range(1, stages))
    return [[0] + far, [0] + far[::-1]]


def step_shapes(factors, order, rows, width):
    left = list(range(len(factors)))[::-1]
    shapes = []
    for axis in order:
        left = [other for other in left if other != axis]
        lead = tuple(factors[other] for other in left)
        shapes.append(((factors[axis] - 1,) + lead + (rows, width), lead + (rows, width)))
    return shapes


class Phase:
    now = None


def phase(name):
    return None


def kernel(
    count, factors, orders, widths, heads,
    tokens_hbm, gates_hbm, lengths_hbm, forget_hbm, gain_hbm, bias_hbm, scale_hbm,
    routes_hbm, shares_hbm, query_hbm, key_hbm, value_hbm, keys_hbm, values_hbm, out_hbm,
    gate_hbm, up_hbm, down_hbm, dense_gate_hbm, dense_up_hbm, dense_down_hbm,
    result_ref, *scratch,
):
    pool = list(scratch)
    take = lambda amount: [pool.pop(0) for _ in range(amount)]
    tokens_ref, gates_ref, lengths_ref, forget_ref, gain_ref, bias_ref, scale_ref = take(7)
    routes_ref, shares_ref, small_sem = take(3)
    gate_ref, up_ref, down_ref, dense_gate_ref, dense_up_ref, dense_down_ref, load_sem = take(7)
    query_weight_ref, key_weight_ref, value_weight_ref, keys_ref, values_ref, early_sem = take(6)
    out_weight_ref, out_sem = take(2)
    query_ref, attended_rows_ref, attended_ref, share_ref, pick_ref, place_ref = take(6)
    mixed_ref, mixed_sem, rows_ref, compact_ref, hidden_ref, dense_ref, settled_ref = take(7)
    cross_start, cross_land, cross_mid, cross_far, cross_sem = take(5)
    stages = len(factors)
    chunks = len(orders)
    per_chunk = []
    for c in range(chunks):
        start = take(1)[0]
        lands = take(stages)
        sums = take(stages - 1)
        per_chunk.append((start, lands, sums))
    exchange_sem = take(1)[0]
    gathered = take(chunks)
    gather_sem = take(1)[0]
    total_rows, model = rows_ref.shape
    seqs = tokens_ref.shape[0]

    me = lax.axis_index("ep")
    coords, strides, rest, stride = [], [], me, 1
    for factor in factors:
        coords.append(lax.rem(rest, factor))
        strides.append(stride)
        rest = rest // factor
        stride *= factor

    def partner(axis, k):
        other = lax.rem(coords[axis] + k, factors[axis])
        return other, me + (other - coords[axis]) * strides[axis]

    def remote(source, target, sems, device):
        return pltpu.make_async_remote_copy(
            src_ref=source, dst_ref=target, send_sem=sems[0], recv_sem=sems[1],
            device_id=(device,), device_id_type=MESH,
        )

    far = factors[-1]
    middle = count // (2 * far)
    core, depth = coords[0], coords[-1]
    place_here = lax.rem(me // 2, middle)
    column = 2 * far
    member = depth * 2 + core

    def across(k):
        other = lax.rem(place_here + k, middle)
        return (depth * middle + other) * 2 + core

    def along(k):
        other = lax.rem(member + k, column)
        return other, ((other // 2) * middle + place_here) * 2 + lax.rem(other, 2)

    barrier = pltpu.get_barrier_semaphore()
    peers = [across(k) for k in range(1, middle)] + [along(k)[1] for k in range(1, column)]

    sources = (gate_hbm, up_hbm, down_hbm, dense_gate_hbm, dense_up_hbm, dense_down_hbm)
    targets = (gate_ref, up_ref, down_ref, dense_gate_ref, dense_up_ref, dense_down_ref)
    loads = [
        pltpu.make_async_copy(source, target, load_sem.at[i])
        for i, (source, target) in enumerate(zip(sources, targets))
    ]
    small = [
        pltpu.make_async_copy(source, target, small_sem.at[i])
        for i, (source, target) in enumerate(
            [
                (tokens_hbm, tokens_ref), (forget_hbm, forget_ref), (gates_hbm, gates_ref),
                (lengths_hbm, lengths_ref), (routes_hbm, routes_ref), (shares_hbm, shares_ref),
                (gain_hbm, gain_ref), (bias_hbm, bias_ref), (scale_hbm, scale_ref),
            ]
        )
    ]
    pieces = 4
    piece = model // pieces
    early = [
        pltpu.make_async_copy(source, target, early_sem.at[i])
        for i, (source, target) in enumerate(
            [(key_hbm, key_weight_ref), (value_hbm, value_weight_ref)]
            + [
                (
                    query_hbm.at[:, pl.ds(i * piece, piece)],
                    query_weight_ref.at[:, pl.ds(i * piece, piece)],
                )
                for i in range(pieces)
            ]
        )
    ]
    batches = 2
    batch = seqs // batches
    caches = [
        [
            pltpu.make_async_copy(
                source.at[pl.ds(i * batch, batch)], target.at[pl.ds(i * batch, batch)],
                early_sem.at[2 + pieces + 2 * i + j],
            )
            for j, (source, target) in enumerate([(keys_hbm, keys_ref), (values_hbm, values_ref)])
        ]
        for i in range(batches)
    ]

    def wait_all(some):
        for copy in some:
            copy.wait()

    out_rows = out_hbm.shape[0]
    own_rows = out_weight_ref.at[pl.ds(pl.multiple_of(place_here * out_rows, out_rows), out_rows)]
    own_out = pltpu.make_async_copy(out_hbm, own_rows, out_sem.at[2])

    small[0].start()
    small[1].start()
    for copy in early:
        copy.start()
    for copy in small[2:]:
        copy.start()
    own_out.start()
    for peer in peers:
        pl.semaphore_signal(barrier, inc=1, device_id=(peer,), device_id_type=MESH)
    for i in range(batches):
        for copy in caches[i]:
            copy.start()

    def spread_out_weight():
        phase("barrier")
        pl.semaphore_wait(barrier, len(peers))
        phase("gather")
        for k in range(1, middle):
            remote(out_hbm, own_rows, (out_sem.at[0], out_sem.at[1]), across(k)).start()

    def wait_small():
        phase("small")
        wait_all(small[:2])
        spread_out_weight()
        phase("gate")

    def wait_keys():
        phase("kv_wait")
        wait_all(early[:2])
        phase("kv")

    def wait_query(i):
        phase("q_wait" + str(i))
        early[2 + i].wait()
        phase("query" + str(i))

    def wait_caches(i):
        phase("cache_wait" + str(i))
        if i == 0:
            wait_all(small[2:4])
        wait_all(caches[i])
        if i == batches - 1:
            for load in loads:
                load.start()
        phase("attn" + str(i))

    waits = {
        "small": wait_small, "keys": wait_keys, "query": wait_query,
        "pieces": pieces, "caches": wait_caches, "batches": batches,
    }
    kv_count = gates_ref.shape[1]
    attend(
        heads, kv_count, tokens_ref, query_weight_ref, key_weight_ref, value_weight_ref,
        forget_ref, keys_ref, values_ref, gates_ref, lengths_ref, query_ref,
        attended_rows_ref, waits, count // heads,
    )
    phase("a2a_start")
    for t in range(column):
        blocks = [
            attended_rows_ref[pl.ds((((t // 2) * middle + m) * 2 + t % 2) * seqs, seqs), :][:, :out_rows]
            for m in range(middle)
        ]
        attended_ref[t] = jnp.concatenate(blocks, axis=1).astype(jnp.bfloat16)
    for k in range(1, column):
        other, device = along(k)
        remote(
            attended_ref.at[other], mixed_ref.at[member], (mixed_sem.at[0], mixed_sem.at[1]), device
        ).start()
    mixed_ref[member] = attended_ref[member]

    phase("share")
    wait_all(small[4:])
    own_expert = me // (count // EXPERTS)
    row_tile = min(total_rows, 256)
    tiles = total_rows // row_tile
    blocks_of = row_tile // seqs
    slots = blocks_of * CAP
    row_of = lax.broadcasted_iota(jnp.int32, (row_tile, row_tile), 0)
    column_of = lax.broadcasted_iota(jnp.int32, (row_tile, row_tile), 1)
    before = jnp.where((row_of // seqs == column_of // seqs) & (row_of < column_of), 1.0, 0.0)
    before = before.astype(jnp.bfloat16)
    slot_of = lax.broadcasted_iota(jnp.int32, (slots, row_tile), 0)
    first_of = lax.broadcasted_iota(jnp.int32, (slots, row_tile), 1) // seqs * CAP
    for i in range(tiles):
        at = slice(i * row_tile, (i + 1) * row_tile)
        matches = routes_ref[:, at] == own_expert
        chosen = jnp.sum(jnp.where(matches, shares_ref[:, at], 0.0), axis=0, keepdims=True)
        hits = jnp.sum(jnp.where(matches, 1.0, 0.0), axis=0, keepdims=True)
        rank = jnp.dot(
            jnp.broadcast_to(hits, (8, row_tile)).astype(jnp.bfloat16), before,
            preferred_element_type=jnp.float32,
        )[0:1]
        wanted = first_of + rank.astype(jnp.int32)
        picked = jnp.where((wanted == slot_of) & (hits > 0.5), 1.0, 0.0)
        share_ref[i * slots:(i + 1) * slots, :] = jnp.sum(picked * chosen, axis=1, keepdims=True)
        pick_ref[i * slots:(i + 1) * slots, :] = picked.astype(jnp.bfloat16)
        place_ref[at, :] = picked.T.astype(jnp.bfloat16)

    def wait_bytes(block, sems, device):
        copy = remote(block, block, sems, device)
        copy.wait()

    phase("a2a_wait")
    wait_bytes(
        mixed_ref.at[pl.ds(0, column - 1)], (mixed_sem.at[0], mixed_sem.at[1]), along(1)[1]
    )
    phase("gather_wait")
    own_out.wait()
    if middle > 1:
        wait_bytes(
            out_weight_ref.at[pl.ds(0, (middle - 1) * out_rows)], (out_sem.at[0], out_sem.at[1]),
            across(1),
        )

    phase("proj")
    left_side = mixed_ref[...].astype(jnp.float32).reshape(column * seqs, middle * out_rows)
    left_side = left_side.astype(jnp.bfloat16)
    halves = cross_start.shape[0]
    half = model // halves
    _, twin = partner(0, 1)
    for h in range(halves):
        part = jnp.dot(
            left_side, out_weight_ref[:, h * half:(h + 1) * half], preferred_element_type=jnp.float32
        )
        part = part.reshape(far, 2, seqs, half).astype(jnp.bfloat16)
        for j in range(2):
            cross_start[h, j] = part[:, j]
        remote(
            cross_start.at[h, 1 - core], cross_land.at[h], (cross_sem.at[0, h, 0], cross_sem.at[0, h, 1]),
            twin,
        ).start()
    phase("rs1a")
    for h in range(halves):
        wait_bytes(cross_land.at[h], (cross_sem.at[0, h, 0], cross_sem.at[0, h, 1]), twin)
        summed = cross_start[h, core].astype(jnp.float32) + cross_land[h].astype(jnp.float32)
        cross_mid[h] = summed.astype(jnp.bfloat16)
        for k in range(far - 1, 0, -1):
            other, device = partner(stages - 1, k)
            remote(
                cross_mid.at[h, other], cross_far.at[h, k - 1],
                (cross_sem.at[1, h, 0], cross_sem.at[1, h, 1]), device,
            ).start()
    phase("rs1b")
    projected = []
    for h in range(halves):
        wait_bytes(cross_far.at[h], (cross_sem.at[1, h, 0], cross_sem.at[1, h, 1]), twin)
        own = cross_mid[h, depth].astype(jnp.float32)
        for k in range(far - 1):
            own = own + cross_far[h, k].astype(jnp.float32)
        projected.append(own)
    projected = jnp.concatenate(projected, axis=-1)
    phase("norm1")
    settled = layer_norm(
        residual_scale * tokens_ref[...].astype(jnp.float32) + projected, gain_ref[0:1], bias_ref[0:1]
    )
    settled_ref[...] = settled

    def at_axis(left, axis, index):
        return tuple(index if other == axis else slice(None) for other in left)

    def exchanger():
        current = [entry[0] for entry in per_chunk]
        left = [list(range(stages))[::-1] for _ in orders]
        finished = [None] * chunks

        def sems(c, stage):
            return exchange_sem.at[c, stage, 0], exchange_sem.at[c, stage, 1]

        def launch(c, stage):
            axis = orders[c][stage]
            for k in range(1, factors[axis]):
                other, device = partner(axis, k)
                remote(
                    current[c].at[at_axis(left[c], axis, other)], per_chunk[c][1][stage].at[k - 1],
                    sems(c, stage), device,
                ).start()

        def advance(c, stage):
            axis = orders[c][stage]
            landed = per_chunk[c][1][stage]
            wait_bytes(landed, sems(c, stage), partner(axis, 1)[1])
            own = current[c][at_axis(left[c], axis, coords[axis])].astype(jnp.float32)
            for k in range(factors[axis] - 1):
                own = own + landed[k].astype(jnp.float32)
            left[c] = [other for other in left[c] if other != axis]
            if stage == stages - 1:
                finished[c] = own
            else:
                current[c] = per_chunk[c][2][stage]
                current[c][...] = own.astype(jnp.bfloat16)
                launch(c, stage + 1)

        def finish():
            for stage in range(stages):
                for c in range(chunks):
                    if stage or c:
                        advance(c, stage)
            return jnp.concatenate(finished, axis=-1)

        def computed(c):
            launch(c, 0)
            if c == 1:
                advance(0, 0)

        return computed, finish

    def place(start_ref, first, value, column, span):
        blocks = value.shape[0] // seqs
        lead = start_ref.shape[:-2]
        flat = value.reshape(blocks, seqs, span).astype(jnp.bfloat16)
        inner = lead[1:]
        size = 1
        for factor in inner:
            size *= factor
        whole = blocks // size
        start_ref[pl.ds(first * whole, whole), ..., column] = flat.reshape((whole,) + inner + (seqs, span))

    phase("ag")
    mine = tuple(coords[axis] for axis in range(stages)[::-1])
    begin = 0
    for c in range(chunks):
        gathered[c][mine] = settled[:, begin:begin + widths[c]]
        begin += widths[c]
    have = [[] for _ in orders]

    def gather_sems(c, stage):
        return gather_sem.at[c, stage, 0], gather_sem.at[c, stage, 1]

    def region(c):
        return tuple(
            slice(None) if other in have[c] else coords[other] for other in range(stages)[::-1]
        )

    def spread(c, stage):
        axis = orders[c][::-1][stage]
        block = gathered[c].at[region(c)]
        for k in range(1, factors[axis]):
            _, device = partner(axis, k)
            remote(block, block, gather_sems(c, stage), device).start()

    def arrive(c, stage):
        axis = orders[c][::-1][stage]
        index = tuple(
            pl.ds(0, factors[other] - 1) if other == axis else (slice(None) if other in have[c] else 0)
            for other in range(stages)[::-1]
        )
        wait_bytes(gathered[c].at[index], gather_sems(c, stage), partner(axis, 1)[1])
        have[c].append(axis)

    for c in range(chunks):
        spread(c, 0)
    for stage in range(stages):
        for c in range(chunks):
            arrive(c, stage)
            if stage < stages - 1:
                spread(c, stage + 1)
    phase("rows")
    begin = 0
    for c in range(chunks):
        block = gathered[c][...].astype(jnp.float32).reshape(total_rows, widths[c])
        rows_ref[:, begin:begin + widths[c]] = block.astype(jnp.bfloat16)
        begin += widths[c]

    phase("pick")
    for i in (0, 1, 3, 4):
        loads[i].wait()
    span = 256
    units = gate_ref.shape[1]
    unit_span = span if units % span == 0 else units

    for i in range(tiles):
        compact_ref[i * slots:(i + 1) * slots, :] = jnp.dot(
            pick_ref[i * slots:(i + 1) * slots, :], rows_ref[i * row_tile:(i + 1) * row_tile, :],
            preferred_element_type=jnp.float32,
        ).astype(jnp.bfloat16)

    def hidden_of(inputs, gates, ups, depth=0):
        contract = (((1,), (depth,)), ((), ()))
        gate_val = lax.dot_general(inputs, gates, contract, preferred_element_type=jnp.float32)
        up_val = lax.dot_general(inputs, ups, contract, preferred_element_type=jnp.float32)
        return (jax.nn.silu(gate_val) * up_val).astype(jnp.bfloat16)

    phase("ffn1d")
    for i in range(tiles):
        at_rows = slice(i * row_tile, (i + 1) * row_tile)
        dense_ref[at_rows, :] = hidden_of(rows_ref[at_rows, :], dense_gate_ref[...], dense_up_ref[...], 1)
    phase("ffn1e")
    for step in range(units // unit_span):
        at_units = slice(step * unit_span, (step + 1) * unit_span)
        hidden_ref[:, at_units] = hidden_of(compact_ref[...], gate_ref[:, at_units], up_ref[:, at_units])

    phase("ffn2")
    for i in (2, 5):
        loads[i].wait()
    computed, finish = exchanger()
    begin = 0
    for c in range(chunks):
        for step in range(widths[c] // span):
            at_columns = slice(begin + step * span, begin + (step + 1) * span)
            expert_out = jnp.dot(
                hidden_ref[...], down_ref[:, at_columns], preferred_element_type=jnp.float32
            )
            expert_out = (share_ref[...] * expert_out).astype(jnp.bfloat16)
            for i in range(tiles):
                at_rows = slice(i * row_tile, (i + 1) * row_tile)
                dense_out = jnp.dot(
                    dense_ref[at_rows, :], dense_down_ref[:, at_columns],
                    preferred_element_type=jnp.float32,
                )
                placed = jnp.dot(
                    place_ref[at_rows, :], expert_out[i * slots:(i + 1) * slots],
                    preferred_element_type=jnp.float32,
                )
                part = placed + scale_ref[:, at_columns] * dense_out
                place(per_chunk[c][0], i, part, pl.ds(step * span, span), span)
        begin += widths[c]
        computed(c)

    phase("rs2")
    ffn = finish()
    phase("norm2")
    result_ref[...] = layer_norm(
        residual_scale * settled_ref[...].astype(jnp.float32) + ffn, gain_ref[1:2], bias_ref[1:2]
    )
    phase(None)


def whole_step(
    count, heads, tokens, gates, lengths, forget, norm_gain, norm_bias, dense_scale, routes, shares,
    query_weight, key_weight, value_weight, cache_keys, cache_values, out_weight,
    expert_gate, expert_up, expert_down, dense_gate, dense_up, dense_down,
):
    seqs, model = tokens.shape
    factors = factors_of(count)
    stages = len(factors)
    orders = orders_of(stages)
    chunks = len(orders)
    narrow = model * 3 // 8
    widths = [model - narrow, narrow]
    total_rows = count * seqs
    lead = tuple(factors[::-1])
    far = factors[-1]
    column = 2 * far
    middle = count // column
    out_rows = out_weight.shape[0]
    row_tile = min(total_rows, 256)
    slots = row_tile // seqs * CAP
    tiles = total_rows // row_tile
    halves = 2
    small = (tokens, gates, lengths, forget, norm_gain, norm_bias, dense_scale, routes, shares)
    scratch = [pltpu.VMEM(array.shape, array.dtype) for array in small]
    scratch += [pltpu.SemaphoreType.DMA((len(small),))]
    scratch += [
        pltpu.VMEM(array.shape, array.dtype)
        for array in (expert_gate, expert_up, expert_down, dense_gate, dense_up, dense_down)
    ]
    scratch += [
        pltpu.SemaphoreType.DMA((6,)),
        *[
            pltpu.VMEM(array.shape, array.dtype)
            for array in (query_weight, key_weight, value_weight, cache_keys, cache_values)
        ],
        pltpu.SemaphoreType.DMA((10,)),
        pltpu.VMEM((middle * out_rows, model), jnp.bfloat16),
        pltpu.SemaphoreType.DMA((3,)),
        pltpu.VMEM((heads * seqs, key_weight.shape[1]), jnp.float32),
        pltpu.VMEM((total_rows, 128), jnp.float32),
        pltpu.VMEM((column, seqs, middle * out_rows), jnp.bfloat16),
        pltpu.VMEM((tiles * slots, 1), jnp.float32),
        pltpu.VMEM((tiles * slots, row_tile), jnp.bfloat16),
        pltpu.VMEM((total_rows, slots), jnp.bfloat16),
        pltpu.VMEM((column, seqs, middle * out_rows), jnp.bfloat16),
        pltpu.SemaphoreType.DMA((2,)),
        pltpu.VMEM((total_rows, model), jnp.bfloat16),
        pltpu.VMEM((tiles * slots, model), jnp.bfloat16),
        pltpu.VMEM((tiles * slots, expert_gate.shape[1]), jnp.bfloat16),
        pltpu.VMEM((total_rows, dense_gate.shape[0]), jnp.bfloat16),
        pltpu.VMEM((seqs, model), jnp.bfloat16),
        pltpu.VMEM((halves, 2, far, seqs, model // halves), jnp.bfloat16),
        pltpu.VMEM((halves, far, seqs, model // halves), jnp.bfloat16),
        pltpu.VMEM((halves, far, seqs, model // halves), jnp.bfloat16),
        pltpu.VMEM((halves, far - 1, seqs, model // halves), jnp.bfloat16),
        pltpu.SemaphoreType.DMA((2, halves, 2)),
    ]
    for order, width in zip(orders, widths):
        shapes = step_shapes(factors, order, seqs, width)
        scratch.append(pltpu.VMEM(lead + (seqs, width), jnp.bfloat16))
        scratch += [pltpu.VMEM(shape[0], jnp.bfloat16) for shape in shapes]
        scratch += [pltpu.VMEM(shape[1], jnp.bfloat16) for shape in shapes[:-1]]
    scratch += [pltpu.SemaphoreType.DMA((chunks, stages, 2))]
    scratch += [pltpu.VMEM(lead + (seqs, width), jnp.bfloat16) for width in widths]
    scratch += [pltpu.SemaphoreType.DMA((chunks, stages, 2))]
    away = pl.BlockSpec(memory_space=pl.ANY)
    return pl.pallas_call(
        functools.partial(kernel, count, factors, orders, widths, heads),
        out_shape=pltpu.VMEM((seqs, model), jnp.bfloat16),
        in_specs=[away] * 21,
        out_specs=pl.BlockSpec(memory_space=pltpu.VMEM),
        scratch_shapes=scratch,
        compiler_params=pltpu.CompilerParams(
            collective_id=0, has_side_effects=True, vmem_limit_bytes=60 * 1024 * 1024
        ),
        name="whole_step",
    )(
        tokens, gates, lengths, forget, norm_gain, norm_bias, dense_scale, routes, shares,
        query_weight, key_weight, value_weight, cache_keys, cache_values, out_weight,
        expert_gate, expert_up, expert_down, dense_gate, dense_up, dense_down,
    )


def local(
    tokens,
    cache_keys,
    cache_values,
    cum_gates,
    lengths,
    query_weight,
    key_weight,
    value_weight,
    forget_weight,
    out_weight,
    norm_gain,
    norm_bias,
    dense_gate_weight,
    dense_up_weight,
    dense_down_weight,
    dense_scale,
    expert_gate_weight,
    expert_up_weight,
    expert_down_weight,
    routes,
    route_weights,
):
    count = lax.axis_size("ep")
    head_dim = key_weight.shape[1] // cum_gates.shape[2]
    heads = query_weight.shape[1] // head_dim
    return whole_step(
        count, heads, tokens, jnp.transpose(cum_gates, (0, 2, 1)), lengths[None, :], forget_weight.T,
        norm_gain, norm_bias, dense_scale[None, :], routes.T, route_weights.T,
        query_weight, key_weight, value_weight, cache_keys, cache_values, out_weight,
        expert_gate_weight, expert_up_weight, expert_down_weight,
        dense_gate_weight.T, dense_up_weight.T, dense_down_weight,
    )


def solution(mesh):
    return jax.shard_map(
        local,
        mesh=mesh,
        in_specs=(
            P("ep", None),
            P("ep", None, None),
            P("ep", None, None),
            P("ep", None, None),
            P("ep"),
            P(),
            P(),
            P(),
            P(),
            P("ep", None),
            P(),
            P(),
            P(None, "ep"),
            P(None, "ep"),
            P("ep", None),
            P(),
            P(None, "ep"),
            P(None, "ep"),
            P("ep", None),
            P(),
            P(),
        ),
        out_specs=P("ep", None),
        check_vma=False,
    )
```

time: 64.4 us -> 54.2 us (0.84)
  Pallas kernels: 62.8 us -> 53.4 us
  local copies, waits for them, and re-layouts: 1.38 us -> 0.62 us
    pallas_call x1, Pallas kernels: 62.8 us -> 53.4 us  [whole_step(): pl.pallas_call(functools.partial(kernel, count, factors, orders, widths,...]
    unnamed x1, local copies, waits for them, and re-layouts: 1.38 us -> 0.62 us
where the time goes in v1:
time: 54.2 us; the launch traced here: 54 us
  Pallas kernels  53.4 us (99%)
  local copies, waits for them, and re-layouts  0.62 us (1%)
    pallas_call x1, Pallas kernels, whole_step(): pl.pallas_call(functools.partial(kernel, count, factors, orders, widths,...  53.4 us

profile of v1, /device:TPU:0, one launch (start us, length us, event | category | flops | bytes accessed | tf_op | source)
XLA Modules:
  0.0 54.0 jit_solution(16156957146611546717)
XLA Ops:
  0.0 53.4 %whole_step.1 = bf16[8,2048]{1,0:T(8,128)(2,1)S(1)} custom-call(bf16[8,2048]{1,0:T(8,128)(2,1)} %tokens_hbm.1, f32[8,2,1024]{2,1,0:T(2,128)} %bitcast.10, s32[1,8]{1,0:T(1,128)} %bitcast.15, bf16[2,2048]{1,0:T(2,128)(2,1)} %bitcast.11, f32[2,2048]{1,0:T(2,128)} %gain_hbm.1, f32[2,2048]{1,0:T(2,128)} %bias_hbm.1, f32[1,2048]{1,0:T(1,128)} %bitcast.12, ...), custom_call_target="tpu_custom_call" | custom-call | tf_op jit(solution)/shard_map/whole_step/pallas_call | solution.py:652
  53.4 0.6 %copy.23 = bf16[8,2048]{1,0:T(8,128)(2,1)} copy(bf16[8,2048]{1,0:T(8,128)(2,1)S(1)} %whole_step.1) | data formatting | bytes 65536
